TPU v7x, 32 devices: a whole 2x2x4 slice. The times are simulated.
32 devices in a mesh: gr: 2 (over y), fs: 4 (over z), tp: 4 (over x, core).
Axes of the slice: x: 2, y: 2, z: 4, core: 2. Of those that a mesh axis runs over, the one named last changes fastest.
Arguments:
- prompt: bfloat16 [4096, 2048], P(('gr', 'fs')), may hold values from -6 to 6
- norm_gain: float32 [2048], P(('gr', 'fs')), may hold values from 0.1 to 1.9
- gate_master: float32 [32, 2048, 1024], P(None, ('gr', 'fs'), 'tp'), may hold values from -6 to 6
- up_master: float32 [32, 2048, 1024], P(None, ('gr', 'fs'), 'tp'), may hold values from -6 to 6
- down_master: float32 [32, 2048, 1024], P(None, ('gr', 'fs'), 'tp'), may hold values from -6 to 6
- routes: int32 [4096, 2], P(('gr', 'fs')), may hold values from 0 to 31, as said below
- route_weights: float32 [4096, 2], P(('gr', 'fs')), may hold values from 0.1 to 0.9
Outputs:
- gate_ready: bfloat16 [32, 2048, 1024], P('fs', None, 'tp')
- up_ready: bfloat16 [32, 2048, 1024], P('fs', None, 'tp')
- down_ready: bfloat16 [32, 2048, 1024], P('fs', None, 'tp')
- blended: bfloat16 [4096, 2048], P(('gr', 'fs'), 'tp')
Inputs may be any that keep to these rules, and one draw needn't show every extreme that they name: `routes`: each row names 2 different experts of one group: expert // 8 is the group. In every aligned block of 512 rows (the tokens of one index of gr and fs) half of the rows choose one group, and no expert is named more than 64 times; in every block some expert is named exactly 64 times.
All inputs are finite; a program needn't handle non-finite values.
Results may differ from a plain program's by a relative error of at most 0.015.
Values may be sent and summed in bfloat16 or wider, within the bound.
A program may use at most 128 MiB of HBM per device.

v0:
```python
import jax
import jax.numpy as jnp
from jax import lax
from jax.sharding import PartitionSpec as P

D = 2048
FF = 1024
EPS = 1e-06


def per_device(prompt, norm_gain, gate_master, up_master, down_master, routes, route_weights):
    gate_low = (norm_gain[None, :, None] * gate_master).astype(jnp.bfloat16)
    up_low = (norm_gain[None, :, None] * up_master).astype(jnp.bfloat16)
    down_low = down_master.astype(jnp.bfloat16)
    experts = gate_low.shape[0]
    fs_count = lax.axis_size("fs")
    local_experts = experts // fs_count
    resharded = (
        lax.all_to_all(gate_low, "fs", split_axis=0, concat_axis=1, tiled=True),
        lax.all_to_all(up_low, "fs", split_axis=0, concat_axis=1, tiled=True),
        lax.all_to_all(down_low, "fs", split_axis=0, concat_axis=1, tiled=True),
    )
    gate_ready, up_ready, down_ready = (
        lax.all_gather(resharded[0], "gr", axis=1, tiled=True),
        lax.all_gather(resharded[1], "gr", axis=1, tiled=True),
        lax.all_gather(resharded[2], "gr", axis=1, tiled=True),
    )
    tokens = prompt.shape[0]
    capacity = tokens // 8
    prompt_wide = prompt.astype(jnp.float32)
    normed = (
        prompt_wide * lax.rsqrt(jnp.mean(prompt_wide * prompt_wide, axis=-1, keepdims=True) + EPS)
    ).astype(jnp.bfloat16)
    route_list = routes.reshape(-1)
    route_hits = (route_list[:, None] == jnp.arange(experts, dtype=jnp.int32)[None, :]).astype(
        jnp.int32
    )
    slot_rank = jnp.sum((jnp.cumsum(route_hits, axis=0) - 1) * route_hits, axis=1)
    slot_index = route_list * capacity + slot_rank
    token_of = jnp.arange(route_list.shape[0], dtype=jnp.int32) // routes.shape[1]
    slot_owner = jnp.zeros((experts * capacity,), jnp.int32).at[slot_index].set(token_of)
    outgoing = normed[slot_owner].reshape(fs_count, local_experts, capacity, normed.shape[1])
    arrived = lax.all_to_all(outgoing, "fs", split_axis=0, concat_axis=0, tiled=True)
    pre_gate = jnp.einsum(
        "secd,edf->secf", arrived, gate_ready, preferred_element_type=jnp.float32
    ) * D ** (-0.5)
    pre_up = jnp.einsum(
        "secd,edf->secf", arrived, up_ready, preferred_element_type=jnp.float32
    ) * D ** (-0.5)
    hidden = (jax.nn.silu(pre_gate) * pre_up).astype(jnp.bfloat16)
    partial_value = (
        jnp.einsum("secf,edf->secd", hidden, down_ready, preferred_element_type=jnp.float32)
        * FF ** (-0.5)
    ).astype(jnp.bfloat16)
    summed = lax.psum_scatter(partial_value, "tp", scatter_dimension=3, tiled=True).astype(
        jnp.float32
    )
    answers = lax.all_to_all(
        summed.astype(jnp.bfloat16), "fs", split_axis=0, concat_axis=0, tiled=True
    )
    answers_flat = answers.reshape(experts * capacity, answers.shape[3])
    picked = answers_flat[slot_index].reshape(tokens, routes.shape[1], answers.shape[3])
    blended = jnp.sum(picked.astype(jnp.float32) * route_weights[:, :, None], axis=1)
    return (gate_ready, up_ready, down_ready, blended.astype(jnp.bfloat16))


def solution(mesh):
    in_specs = (
        P(("gr", "fs"), None),
        P(("gr", "fs")),
        P(None, ("gr", "fs"), "tp"),
        P(None, ("gr", "fs"), "tp"),
        P(None, ("gr", "fs"), "tp"),
        P(("gr", "fs"), None),
        P(("gr", "fs"), None),
    )
    out_specs = (
        P("fs", None, "tp"),
        P("fs", None, "tp"),
        P("fs", None, "tp"),
        P(("gr", "fs"), "tp"),
    )
    return jax.shard_map(
        per_device, mesh=mesh, in_specs=in_specs, out_specs=out_specs, check_vma=False
    )
```

profile of v0, /device:TPU:0, one launch (start us, length us, event | category | flops | bytes accessed | tf_op | source)
XLA Modules:
  0.0 691.8 jit_solution(8240424116408428662)
XLA Ops:
  7.2 11.5 %multiply_convert_fusion.1 = (bf16[32,256,256]{2,1,0:T(8,128)(2,1)}, bf16[32,256,256]{2,1,0:T(8,128)(2,1)}) fusion(f32[32,256,256]{2,1,0:T(8,128)} %param.10, f32[256]{0:T(256)} %param.8, f32[32,256,256]{2,1,0:T(8,128)} %param.9), kind=kLoop, calls=%fused_computation.11 | loop fusion | flops 8388608 | bytes 25166848 | tf_op jit(solution)/shard_map/convert_element_type | solution.py:13
  18.7 100.6 %all_to_all.64 = bf16[32,256,256]{2,1,0:T(8,128)(2,1)} all-to-all(bf16[32,256,256]{2,1,0:T(8,128)(2,1)} %get-tuple-element.4), channel_id=1, replica_groups=mesh['gr'=2,'fs'=4,'tp'=4] {'fs'}, dimensions={0} | all-to-all | bytes 8388608 | tf_op jit(solution)/shard_map/all_to_all | solution.py:20
  119.2 4.9 all-to-all-start
  124.2 4.6 copy.27
  128.9 5.9 convert_element_type.42
  134.8 82.3 %all-to-all-done = bf16[32,256,256]{2,1,0:T(8,128)(2,1)} async-done(((bf16[32,256,256]{2,1,0:T(8,128)(2,1)}), bf16[32,256,256]{2,1,0:T(8,128)(2,1)}, u32[]{:S(2)}, u32[]{:S(2)}) %all-to-all-start) | async-done | bytes 4194336 | tf_op jit(solution)/shard_map/all_to_all | solution.py:19
  217.0 4.8 all-to-all-start.2
  221.9 4.6 copy.26
  226.6 0.7 copy-done.1
  227.8 9.0 %reduce-window.6 = s32[32,8,128]{2,1,0:T(8,128)S(1)} reduce-window(s32[32,8,128]{2,1,0:T(8,128)S(1)} %fusion.29, s32[]{:T(128)} %constant.36.clone.1), window={size=1x1x128 pad=0_0x0_0x127_0}, to_apply=%region_1.0 | reduce-window | flops 4161536 | bytes 262148 | tf_op jit(solution)/shard_map/reduce-window
  237.3 0.2 mul.86
  237.7 4.3 scatter_custom_fusion
  242.0 0.5 fusion.9
  242.5 2.3 fusion.10
  244.8 10.9 %gather_fusion = bf16[2048,2048]{1,0:T(8,128)(2,1)} fusion(bf16[512,2048]{1,0:T(8,128)(2,1)S(1)} %fusion.10, s32[2048]{0:T(1024)S(1)} %fusion.30), kind=kCustom, calls=%fused_computation | custom fusion | bytes 16785408 | tf_op jit(solution)/shard_map/gather | solution.py:42
  255.7 58.9 %all-to-all-done.2 = bf16[32,256,256]{2,1,0:T(8,128)(2,1)} async-done(((bf16[32,256,256]{2,1,0:T(8,128)(2,1)}), bf16[32,256,256]{2,1,0:T(8,128)(2,1)}, u32[]{:S(2)}, u32[]{:S(2)}) %all-to-all-start.2) | async-done | bytes 4194336 | tf_op jit(solution)/shard_map/all_to_all | solution.py:21
  314.6 5.7 all-to-all-start.3
  320.4 4.7 copy.28
  325.1 0.2 reduce-scatter.2.cloned.1.call-start
  325.3 177.6 %all-to-all-done.3 = bf16[4,8,64,2048]{3,2,1,0:T(8,128)(2,1)} async-done(((bf16[4,8,64,2048]{3,2,1,0:T(8,128)(2,1)}), bf16[4,8,64,2048]{3,2,1,0:T(8,128)(2,1)}, u32[]{:S(2)}, u32[]{:S(2)}) %all-to-all-start.3) | async-done | bytes 8388640 | tf_op jit(solution)/shard_map/all_to_all | solution.py:43
  502.9 8.1 %fusion.3 = f32[8,256,4,64]{1,3,2,0:T(8,128)S(1)} fusion(bf16[8,2048,256]{2,1,0:T(8,128)(2,1)} %all-gather.6.cloned.1.call-done, bf16[4,8,64,2048]{3,2,1,0:T(8,128)(2,1)} %all-to-all-done.3), kind=kOutput, calls=%fused_computation.7 | convolution fusion | flops 2147483648 | bytes 18874368 | tf_op jit(solution)/shard_map/secd,edf->secf/dot_general | solution.py:47
  511.1 17.0 %fusion = bf16[4,8,64,2048]{3,2,0,1:T(8,128)(2,1)} fusion(bf16[8,2048,256]{2,1,0:T(8,128)(2,1)} %all-gather.8.cloned.1.call-done, f32[8,256,4,64]{1,3,2,0:T(8,128)S(1)} %fusion.3, bf16[4,8,64,2048]{3,2,1,0:T(8,128)(2,1)} %all-to-all-done.3, bf16[8,2048,256]{2,1,0:T(8,128)(2,1)} %all-gather.4.cloned.1.call-done), kind=kOutput, calls=%fused_computation.4 | convolution fusion | flops 4307550208 | bytes 35651584 | tf_op jit(solution)/shard_map/secf,edf->secd/dot_general | solution.py:52
  528.2 70.0 %reduce-scatter.2.cloned.1.call-done = bf16[4,8,64,512]{3,2,0,1:T(8,128)(2,1)} async-done(((bf16[4,8,64,2048]{3,2,0,1:T(8,128)(2,1)}), bf16[4,8,64,512]{3,2,0,1:T(8,128)(2,1)}) %reduce-scatter.2.cloned.1.call-update) | async-done | bytes 2097168 | tf_op jit(solution)/shard_map/reduce_scatter | solution.py:55
  598.2 3.1 copy.36
  601.3 4.6 all-to-all-start.4
  606.1 47.9 %all-to-all-done.4 = bf16[4,8,64,512]{3,2,1,0:T(8,128)(2,1)S(1)} async-done(((bf16[4,8,64,512]{3,2,1,0:T(8,128)(2,1)}), bf16[4,8,64,512]{3,2,1,0:T(8,128)(2,1)S(1)}, u32[]{:S(2)}, u32[]{:S(2)}) %all-to-all-start.4) | async-done | bytes 2097184 | tf_op jit(solution)/shard_map/all_to_all | solution.py:58
  653.9 4.0 gather_fusion.1
  657.9 1.3 reshape.78
  659.3 4.0 multiply_reduce_fusion
  663.3 7.3 %copy.54 = bf16[8,2048,256]{2,1,0:T(8,128)(2,1)} copy(bf16[8,2048,256]{2,1,0:T(8,128)(2,1)} %all-gather.4.cloned.1.call-done) | data formatting | bytes 16777216
  670.6 7.3 %copy.55 = bf16[8,2048,256]{2,1,0:T(8,128)(2,1)} copy(bf16[8,2048,256]{2,1,0:T(8,128)(2,1)} %all-gather.6.cloned.1.call-done) | data formatting | bytes 16777216
  677.9 7.3 %copy.56 = bf16[8,2048,256]{2,1,0:T(8,128)(2,1)} copy(bf16[8,2048,256]{2,1,0:T(8,128)(2,1)} %all-gather.8.cloned.1.call-done) | data formatting | bytes 16777216
  (34 shorter events, 1.5 us)
Async XLA Ops:
  119.2 97.8 %all-to-all-start = ((bf16[32,256,256]{2,1,0:T(8,128)(2,1)}), bf16[32,256,256]{2,1,0:T(8,128)(2,1)}, u32[]{:S(2)}, u32[]{:S(2)}) async-start(bf16[32,256,256]{2,1,0:T(8,128)(2,1)} %get-tuple-element.5), calls=%async_computation | async-start | bytes 8388608 | tf_op jit(solution)/shard_map/all_to_all | solution.py:19
  124.1 378.8 %all-gather.6.cloned.1.call-start = ((), (), s32[]{:S(2)}) async-start(), calls=%async_computation.7 | async-start | bytes 12582912 | tf_op jit(solution)/shard_map/all_gather | solution.py:25
  217.0 97.6 %all-to-all-start.2 = ((bf16[32,256,256]{2,1,0:T(8,128)(2,1)}), bf16[32,256,256]{2,1,0:T(8,128)(2,1)}, u32[]{:S(2)}, u32[]{:S(2)}) async-start(bf16[32,256,256]{2,1,0:T(8,128)(2,1)} %convert_element_type.42), calls=%async_computation.2 | async-start | bytes 8388608 | tf_op jit(solution)/shard_map/all_to_all | solution.py:21
  221.9 289.2 %all-gather.4.cloned.1.call-start = ((), (), s32[]{:S(2)}) async-start(), calls=%async_computation.6 | async-start | bytes 12582912 | tf_op jit(solution)/shard_map/all_gather | solution.py:24
  226.6 0.7 copy-start.1
  226.6 15.4 %copy-start = (bf16[512,2048]{1,0:T(8,128)(2,1)S(1)}, bf16[512,2048]{1,0:T(8,128)(2,1)}, u32[]{:S(2)}) copy-start(bf16[512,2048]{1,0:T(8,128)(2,1)} %param.7) | copy-start | bytes 6291460
  314.6 188.3 %all-to-all-start.3 = ((bf16[4,8,64,2048]{3,2,1,0:T(8,128)(2,1)}), bf16[4,8,64,2048]{3,2,1,0:T(8,128)(2,1)}, u32[]{:S(2)}, u32[]{:S(2)}) async-start(bf16[4,8,64,2048]{3,2,1,0:T(8,128)(2,1)} %bitcast.75), calls=%async_computation.3 | async-start | bytes 16777216 | tf_op jit(solution)/shard_map/all_to_all | solution.py:43
  320.3 190.8 %all-gather.8.cloned.1.call-start = ((), (), s32[]{:S(2)}) async-start(), calls=%async_computation.8 | async-start | bytes 12582912 | tf_op jit(solution)/shard_map/all_gather | solution.py:26
  325.1 273.1 %reduce-scatter.2.cloned.1.call-start = ((), (), s32[]{:S(2)}) async-start(), calls=%async_computation.9 | async-start | bytes 10485760 | tf_op jit(solution)/shard_map/reduce_scatter | solution.py:55
  528.2 77.8 %copy-start.2 = (f32[512,2]{0,1:T(2,128)S(1)}, f32[512,2]{0,1:T(2,128)}, u32[]{:S(2)}) copy-start(f32[512,2]{0,1:T(2,128)} %param.13) | copy-start | bytes 12292
  601.3 52.6 %all-to-all-start.4 = ((bf16[4,8,64,512]{3,2,1,0:T(8,128)(2,1)}), bf16[4,8,64,512]{3,2,1,0:T(8,128)(2,1)S(1)}, u32[]{:S(2)}, u32[]{:S(2)}) async-start(bf16[4,8,64,512]{3,2,1,0:T(8,128)(2,1)} %copy.36), calls=%async_computation.5 | async-start | bytes 4194304 | tf_op jit(solution)/shard_map/all_to_all | solution.py:58
Sparse Core Ops, SparseCore 0:
  129.0 105.3 all-gather.5
  236.5 103.9 all-gather.3
  342.1 103.9 all-gather.7
  528.3 69.8 reduce-scatter.1
where the time goes:
time: 693 us; the launch traced here: 692 us
  waiting for transfers between devices  437 us (63%)
  blocking collectives  101 us (15%)
  local copies, waits for them, and re-layouts  61.4 us (9%)
  other arithmetic  33.5 us (5%)
  matrix products  25.1 us (4%)
  starting transfers between devices  20.4 us (3%)
  between operations  14 us (2%)
    all_to_all x1, waiting for transfers between devices, per_device(): lax.all_to_all(outgoing, 'fs', split_axis=0, concat_axis=0, tiled=True)  178 us
    all_to_all x1, blocking collectives, per_device(): lax.all_to_all(up_low, 'fs', split_axis=0, concat_axis=1, tiled=True)  101 us
    all_to_all x1, waiting for transfers between devices, per_device(): lax.all_to_all(gate_low, 'fs', split_axis=0, concat_axis=1, tiled=True)  82.3 us
    reduce_scatter x1, waiting for transfers between devices, per_device(): lax.psum_scatter(partial_value, 'tp', scatter_dimension=3, tiled=True)  70 us
    all_to_all x1, waiting for transfers between devices, per_device(): lax.all_to_all(down_low, 'fs', split_axis=0, concat_axis=1, tiled=True)  58.9 us
    all_to_all x1, waiting for transfers between devices, per_device(): lax.all_to_all(summed.astype(jnp.bfloat16), 'fs', split_axis=0, concat_ax...  47.9 us
    unnamed x11, local copies, waits for them, and re-layouts  22.9 us
    dot_general x1, matrix products, per_device(): jnp.einsum('secf,edf->secd', hidden, down_ready, preferred_element_type=j...  17 us
  transfers between devices with their start and end apart: 8, of which 5 were waited for; matrix products, arithmetic and copies ran while one was open for 8% of the time, Pallas kernels for 0%

commit v1 on v0

--- a/solution.py
+++ b/solution.py
@@ -6,6 +6,16 @@
 D = 2048
 FF = 1024
 EPS = 1e-06
+
+
+def bench_answer(local_block, comm_axis):
+    carry = lax.all_to_all(
+        jnp.stack(jnp.split(local_block, lax.axis_size(comm_axis), 0)),
+        axis_name=comm_axis,
+        split_axis=0,
+        concat_axis=0,
+    )
+    return jnp.concatenate(carry, 1)
 
 
 def per_device(prompt, norm_gain, gate_master, up_master, down_master, routes, route_weights):
@@ -17,7 +27,7 @@
     local_experts = experts // fs_count
     resharded = (
         lax.all_to_all(gate_low, "fs", split_axis=0, concat_axis=1, tiled=True),
-        lax.all_to_all(up_low, "fs", split_axis=0, concat_axis=1, tiled=True),
+        bench_answer(up_low, "fs"),
         lax.all_to_all(down_low, "fs", split_axis=0, concat_axis=1, tiled=True),
     )
     gate_ready, up_ready, down_ready = (

time: 693 us -> 695 us (level)
  no operation moved by 1% of the time
where the time goes in v1:
time: 695 us; the launch traced here: 694 us
  waiting for transfers between devices  437 us (63%)
  blocking collectives  99.4 us (14%)
  local copies, waits for them, and re-layouts  64 us (9%)
  other arithmetic  34.1 us (5%)
  matrix products  25.1 us (4%)
  starting transfers between devices  20.4 us (3%)
  between operations  14 us (2%)
    all_to_all x1, waiting for transfers between devices, per_device(): lax.all_to_all(outgoing, 'fs', split_axis=0, concat_axis=0, tiled=True)  178 us
    all_to_all x1, blocking collectives, bench_answer(): lax.all_to_all(jnp.stack(jnp.split(local_block, lax.axis_size(comm_axis),...  99.4 us
    all_to_all x1, waiting for transfers between devices, per_device(): lax.all_to_all(gate_low, 'fs', split_axis=0, concat_axis=1, tiled=True)  81.8 us
    reduce_scatter x1, waiting for transfers between devices, per_device(): lax.psum_scatter(partial_value, 'tp', scatter_dimension=3, tiled=True)  70.4 us
    all_to_all x1, waiting for transfers between devices, per_device(): lax.all_to_all(down_low, 'fs', split_axis=0, concat_axis=1, tiled=True)  58.9 us
    all_to_all x1, waiting for transfers between devices, per_device(): lax.all_to_all(summed.astype(jnp.bfloat16), 'fs', split_axis=0, concat_ax...  47.8 us
    unnamed x11, local copies, waits for them, and re-layouts  22.9 us
    dot_general x1, matrix products, per_device(): jnp.einsum('secf,edf->secd', hidden, down_ready, preferred_element_type=j...  17 us
  transfers between devices with their start and end apart: 8, of which 5 were waited for; matrix products, arithmetic and copies ran while one was open for 8% of the time, Pallas kernels for 0%

profile of v1, /device:TPU:0, one launch (start us, length us, event | category | flops | bytes accessed | tf_op | source)
XLA Modules:
  0.0 693.7 jit_solution(2288694139463486758)
XLA Ops:
  7.2 11.5 %multiply_convert_fusion.1 = (bf16[32,256,256]{2,1,0:T(8,128)(2,1)}, bf16[32,256,256]{2,1,0:T(8,128)(2,1)}) fusion(f32[32,256,256]{2,1,0:T(8,128)} %param.10, f32[256]{0:T(256)} %param.8, f32[32,256,256]{2,1,0:T(8,128)} %param.9), kind=kLoop, calls=%fused_computation.11 | loop fusion | flops 8388608 | bytes 25166848 | tf_op jit(solution)/shard_map/convert_element_type | solution.py:23
  18.7 2.6 slice_bitcast_fusion.3
  21.3 0.6 pad_maximum_fusion
  21.9 99.4 %all_to_all.51 = bf16[4,8,256,256]{3,2,1,0:T(8,128)(2,1)} all-to-all(bf16[4,8,256,256]{3,2,1,0:T(8,128)(2,1)S(1)} %pad_maximum_fusion), channel_id=1, replica_groups=mesh['gr'=2,'fs'=4,'tp'=4] {'fs'}, dimensions={0} | all-to-all | bytes 8388608 | tf_op jit(solution)/shard_map/all_to_all | solution.py:12
  121.2 4.9 all-to-all-start
  126.2 4.6 copy.27
  130.9 5.9 convert_element_type.42
  136.8 81.8 %all-to-all-done = bf16[32,256,256]{2,1,0:T(8,128)(2,1)} async-done(((bf16[32,256,256]{2,1,0:T(8,128)(2,1)}), bf16[32,256,256]{2,1,0:T(8,128)(2,1)}, u32[]{:S(2)}, u32[]{:S(2)}) %all-to-all-start) | async-done | bytes 4194336 | tf_op jit(solution)/shard_map/all_to_all | solution.py:29
  218.6 4.8 all-to-all-start.2
  223.5 4.6 copy.26
  228.1 0.7 copy-done.1
  229.3 9.0 %reduce-window.6 = s32[32,8,128]{2,1,0:T(8,128)S(1)} reduce-window(s32[32,8,128]{2,1,0:T(8,128)S(1)} %fusion.29, s32[]{:T(128)} %constant.36.clone.1), window={size=1x1x128 pad=0_0x0_0x127_0}, to_apply=%region_1.0 | reduce-window | flops 4161536 | bytes 262148 | tf_op jit(solution)/shard_map/reduce-window
  239.2 4.3 scatter_custom_fusion
  243.5 0.5 fusion.9
  244.0 2.3 fusion.10
  246.4 10.9 %gather_fusion = bf16[2048,2048]{1,0:T(8,128)(2,1)} fusion(bf16[512,2048]{1,0:T(8,128)(2,1)S(1)} %fusion.10, s32[2048]{0:T(1024)S(1)} %fusion.30), kind=kCustom, calls=%fused_computation | custom fusion | bytes 16785408 | tf_op jit(solution)/shard_map/gather | solution.py:52
  257.2 58.9 %all-to-all-done.2 = bf16[32,256,256]{2,1,0:T(8,128)(2,1)} async-done(((bf16[32,256,256]{2,1,0:T(8,128)(2,1)}), bf16[32,256,256]{2,1,0:T(8,128)(2,1)}, u32[]{:S(2)}, u32[]{:S(2)}) %all-to-all-start.2) | async-done | bytes 4194336 | tf_op jit(solution)/shard_map/all_to_all | solution.py:31
  316.2 5.7 all-to-all-start.3
  321.9 4.7 copy.28
  326.8 177.7 %all-to-all-done.3 = bf16[4,8,64,2048]{3,2,1,0:T(8,128)(2,1)} async-done(((bf16[4,8,64,2048]{3,2,1,0:T(8,128)(2,1)}), bf16[4,8,64,2048]{3,2,1,0:T(8,128)(2,1)}, u32[]{:S(2)}, u32[]{:S(2)}) %all-to-all-start.3) | async-done | bytes 8388640 | tf_op jit(solution)/shard_map/all_to_all | solution.py:53
  504.5 8.1 %fusion.3 = f32[8,256,4,64]{1,3,2,0:T(8,128)S(1)} fusion(bf16[8,2048,256]{2,1,0:T(8,128)(2,1)} %all-gather.6.cloned.1.call-done, bf16[4,8,64,2048]{3,2,1,0:T(8,128)(2,1)} %all-to-all-done.3), kind=kOutput, calls=%fused_computation.7 | convolution fusion | flops 2147483648 | bytes 18874368 | tf_op jit(solution)/shard_map/secd,edf->secf/dot_general | solution.py:57
  512.6 17.0 %fusion = bf16[4,8,64,2048]{3,2,0,1:T(8,128)(2,1)} fusion(bf16[8,2048,256]{2,1,0:T(8,128)(2,1)} %all-gather.8.cloned.1.call-done, f32[8,256,4,64]{1,3,2,0:T(8,128)S(1)} %fusion.3, bf16[4,8,64,2048]{3,2,1,0:T(8,128)(2,1)} %all-to-all-done.3, bf16[8,2048,256]{2,1,0:T(8,128)(2,1)} %all-gather.4.cloned.1.call-done), kind=kOutput, calls=%fused_computation.4 | convolution fusion | flops 4307550208 | bytes 35651584 | tf_op jit(solution)/shard_map/secf,edf->secd/dot_general | solution.py:62
  529.7 70.4 %reduce-scatter.2.cloned.1.call-done = bf16[4,8,64,512]{3,2,0,1:T(8,128)(2,1)} async-done(((bf16[4,8,64,2048]{3,2,0,1:T(8,128)(2,1)}), bf16[4,8,64,512]{3,2,0,1:T(8,128)(2,1)}) %reduce-scatter.2.cloned.1.call-update) | async-done | bytes 2097168 | tf_op jit(solution)/shard_map/reduce_scatter | solution.py:65
  600.2 3.1 copy.36
  603.3 4.6 all-to-all-start.4
  608.1 47.8 %all-to-all-done.4 = bf16[4,8,64,512]{3,2,1,0:T(8,128)(2,1)S(1)} async-done(((bf16[4,8,64,512]{3,2,1,0:T(8,128)(2,1)}), bf16[4,8,64,512]{3,2,1,0:T(8,128)(2,1)S(1)}, u32[]{:S(2)}, u32[]{:S(2)}) %all-to-all-start.4) | async-done | bytes 2097184 | tf_op jit(solution)/shard_map/all_to_all | solution.py:68
  655.9 4.0 gather_fusion.1
  659.9 1.3 reshape.86
  661.2 4.0 multiply_reduce_fusion
  665.3 7.3 %copy.54 = bf16[8,2048,256]{2,1,0:T(8,128)(2,1)} copy(bf16[8,2048,256]{2,1,0:T(8,128)(2,1)} %all-gather.4.cloned.1.call-done) | data formatting | bytes 16777216
  672.6 7.3 %copy.55 = bf16[8,2048,256]{2,1,0:T(8,128)(2,1)} copy(bf16[8,2048,256]{2,1,0:T(8,128)(2,1)} %all-gather.6.cloned.1.call-done) | data formatting | bytes 16777216
  679.9 7.3 %copy.56 = bf16[8,2048,256]{2,1,0:T(8,128)(2,1)} copy(bf16[8,2048,256]{2,1,0:T(8,128)(2,1)} %all-gather.8.cloned.1.call-done) | data formatting | bytes 16777216
  (36 shorter events, 1.9 us)
Async XLA Ops:
  121.2 97.3 %all-to-all-start = ((bf16[32,256,256]{2,1,0:T(8,128)(2,1)}), bf16[32,256,256]{2,1,0:T(8,128)(2,1)}, u32[]{:S(2)}, u32[]{:S(2)}) async-start(bf16[32,256,256]{2,1,0:T(8,128)(2,1)} %get-tuple-element.9), calls=%async_computation | async-start | bytes 8388608 | tf_op jit(solution)/shard_map/all_to_all | solution.py:29
  126.2 378.3 %all-gather.6.cloned.1.call-start = ((), (), s32[]{:S(2)}) async-start(), calls=%async_computation.7 | async-start | bytes 12582912 | tf_op jit(solution)/shard_map/all_gather | solution.py:35
  218.6 97.6 %all-to-all-start.2 = ((bf16[32,256,256]{2,1,0:T(8,128)(2,1)}), bf16[32,256,256]{2,1,0:T(8,128)(2,1)}, u32[]{:S(2)}, u32[]{:S(2)}) async-start(bf16[32,256,256]{2,1,0:T(8,128)(2,1)} %convert_element_type.42), calls=%async_computation.2 | async-start | bytes 8388608 | tf_op jit(solution)/shard_map/all_to_all | solution.py:31
  223.4 289.2 %all-gather.4.cloned.1.call-start = ((), (), s32[]{:S(2)}) async-start(), calls=%async_computation.6 | async-start | bytes 12582912 | tf_op jit(solution)/shard_map/all_gather | solution.py:34
  228.1 0.7 copy-start.1
  228.1 15.4 %copy-start = (bf16[512,2048]{1,0:T(8,128)(2,1)S(1)}, bf16[512,2048]{1,0:T(8,128)(2,1)}, u32[]{:S(2)}) copy-start(bf16[512,2048]{1,0:T(8,128)(2,1)} %param.7) | copy-start | bytes 6291460
  316.2 188.3 %all-to-all-start.3 = ((bf16[4,8,64,2048]{3,2,1,0:T(8,128)(2,1)}), bf16[4,8,64,2048]{3,2,1,0:T(8,128)(2,1)}, u32[]{:S(2)}, u32[]{:S(2)}) async-start(bf16[4,8,64,2048]{3,2,1,0:T(8,128)(2,1)} %bitcast.81), calls=%async_computation.3 | async-start | bytes 16777216 | tf_op jit(solution)/shard_map/all_to_all | solution.py:53
  321.8 190.8 %all-gather.8.cloned.1.call-start = ((), (), s32[]{:S(2)}) async-start(), calls=%async_computation.8 | async-start | bytes 12582912 | tf_op jit(solution)/shard_map/all_gather | solution.py:36
  326.6 273.6 %reduce-scatter.2.cloned.1.call-start = ((), (), s32[]{:S(2)}) async-start(), calls=%async_computation.9 | async-start | bytes 10485760 | tf_op jit(solution)/shard_map/reduce_scatter | solution.py:65
  529.7 78.2 %copy-start.2 = (f32[512,2]{0,1:T(2,128)S(1)}, f32[512,2]{0,1:T(2,128)}, u32[]{:S(2)}) copy-start(f32[512,2]{0,1:T(2,128)} %param.13) | copy-start | bytes 12292
  603.3 52.6 %all-to-all-start.4 = ((bf16[4,8,64,512]{3,2,1,0:T(8,128)(2,1)}), bf16[4,8,64,512]{3,2,1,0:T(8,128)(2,1)S(1)}, u32[]{:S(2)}, u32[]{:S(2)}) async-start(bf16[4,8,64,512]{3,2,1,0:T(8,128)(2,1)} %copy.36), calls=%async_computation.5 | async-start | bytes 4194304 | tf_op jit(solution)/shard_map/all_to_all | solution.py:68
Sparse Core Ops, SparseCore 0:
  131.0 105.3 all-gather.5
  238.5 103.9 all-gather.3
  344.1 103.9 all-gather.7
  529.8 70.2 reduce-scatter.1
